TPU v7x, 32 devices: a whole 2x2x4 slice. The times are simulated.
32 devices in a mesh: sp: 8 (over z, x), tp: 4 (over y, core).
Axes of the slice: x: 2, y: 2, z: 4, core: 2. Of those that a mesh axis runs over, the one named last changes fastest.
Arguments:
- conv_value: bfloat16 [4096, 1024], P('sp', 'tp'), may hold values from -6 to 6
- conv_gate: bfloat16 [4096, 1024], P('sp', 'tp'), may hold values from -9 to 9
- conv_weight: float32 [31, 1024], P(None, 'tp'), may hold values from -2.2 to 2.2
- conv_gain: float32 [1024], P('tp'), may hold values from 0.1 to 1.9
- conv_shift: float32 [1024], P('tp'), may hold values from -3 to 3
- out_weight: bfloat16 [1024, 2048], P('tp'), may hold values from -0.1875 to 0.1875
- residual: bfloat16 [4096, 2048], P('sp', 'tp'), may hold values from -10 to 10
- mix_gain: float32 [2048], P('tp'), may hold values from 0.1 to 1.9
- expert_ids: int32 [4096, 2], P('sp'), may hold values from 0 to 7, all different within a row; in each aligned block of 128 rows (0 to 127, 128 to 255, ...) at most 64 rows name the same one
- group_weight: float32 [4096], P('sp'), may hold values from 0.6 to 1
- score_gap: float32 [4096], P('sp'), may hold values from -0.8 to 0.8
- w_gate: bfloat16 [8, 2048, 1024], P('sp', None, 'tp'), may hold values from -0.125 to 0.125
- w_up: bfloat16 [8, 2048, 1024], P('sp', None, 'tp'), may hold values from -0.125 to 0.125
- w_down: bfloat16 [8, 1024, 2048], P('sp', 'tp'), may hold values from -0.1875 to 0.1875
Outputs:
- layer_out: bfloat16 [4096, 2048], P('sp', 'tp')
Inputs may be any that keep to these rules, and one draw needn't show every extreme that they name: `expert_ids`: the two experts of a position differ. In each aligned block of 512 // 4 positions no expert is named by more than 64 rows, a bound that some block reaches.
All inputs are finite; a program needn't handle non-finite values.
Results may differ from a plain program's by a relative error of at most 0.012.
Values may be sent and summed in bfloat16 or wider, within the bound.
No kernel may reach another device: no remote copies, remote signals or barrier semaphores. Data moves between devices by JAX's collectives and lax.ppermute only.
A program may use at most 128 MiB of HBM per device.

v0:
```python
import jax
import jax.numpy as jnp
from jax import lax
from jax.sharding import PartitionSpec as P

D = 2048
CH = 1024
eps = 1e-06


def passed_along(value, axis, steps):
    count = lax.axis_size(axis)
    leading, last = (max(0, -steps), min(count, count - steps))
    return lax.ppermute(value, axis, [(source, source + steps) for source in range(leading, last)])


def shards(
    conv_value,
    conv_gate,
    conv_weight,
    conv_gain,
    conv_shift,
    out_weight,
    residual,
    mix_gain,
    expert_ids,
    group_weight,
    score_gap,
    w_gate,
    w_up,
    w_down,
):
    row_count = conv_value.shape[0]
    reach_rows = conv_weight.shape[0] - 1
    seq_devices = lax.axis_size("sp")
    tp_devices = lax.axis_size("tp")
    prev_value, prev_gate = passed_along(
        (conv_value[row_count - reach_rows :], conv_gate[row_count - reach_rows :]), "sp", 1
    )
    values = jnp.concatenate([prev_value, conv_value], axis=0).astype(jnp.float32)
    gate_pre = jnp.concatenate([prev_gate, conv_gate], axis=0).astype(jnp.float32)
    gated = values * jax.nn.sigmoid(gate_pre)
    convolved = jnp.zeros((row_count, conv_value.shape[1]), jnp.float32)
    for tap_index in range(reach_rows + 1):
        convolved = convolved + conv_weight[tap_index] * gated[tap_index : tap_index + row_count]
    row_sum, squares = lax.psum(
        (jnp.sum(convolved, axis=-1), jnp.sum(convolved * convolved, axis=-1)), "tp"
    )
    row_mean = (row_sum / CH)[:, None]
    row_var = (squares / CH)[:, None] - row_mean * row_mean
    normalized = (convolved - row_mean) * lax.rsqrt(row_var + eps) * conv_gain + conv_shift
    activated = jax.nn.silu(normalized).astype(jnp.bfloat16)
    partial_out = jnp.dot(activated, out_weight, preferred_element_type=jnp.float32)
    mixed = lax.psum_scatter(
        partial_out.astype(jnp.bfloat16), "tp", scatter_dimension=1, tiled=True
    ).astype(jnp.float32)
    middle = (residual.astype(jnp.float32) + mixed).astype(jnp.bfloat16)
    middle_wide = middle.astype(jnp.float32)
    row_sq = lax.psum(jnp.sum(middle_wide * middle_wide, axis=-1), "tp")
    normed = (middle_wide * lax.rsqrt(row_sq / D + eps)[:, None] * mix_gain).astype(jnp.bfloat16)
    quarter = row_count // tp_devices
    capacity = 4 * quarter // seq_devices
    expert_num = expert_ids.reshape(tp_devices, quarter * 2)
    onehot = (
        expert_num[:, :, None] == jnp.arange(seq_devices, dtype=jnp.int32)[None, None, :]
    ).astype(jnp.int32)
    before = jnp.cumsum(onehot, axis=1) - onehot
    ranking = jnp.sum(before * onehot, axis=-1)
    quarter_index = jnp.arange(tp_devices, dtype=jnp.int32)[:, None]
    slots = ((expert_num * tp_devices + quarter_index) * capacity + ranking).reshape(-1)
    own_rows = lax.all_to_all(normed, "tp", split_axis=0, concat_axis=1, tiled=True)
    my_index = lax.axis_index("tp")
    own_experts = lax.dynamic_slice_in_dim(expert_num, my_index, 1, 0)[0]
    own_rank = lax.dynamic_slice_in_dim(ranking, my_index, 1, 0)[0]
    own_slots = own_experts * capacity + own_rank
    token_of = jnp.arange(quarter * 2, dtype=jnp.int32) // 2
    outgoing = (
        jnp.zeros((seq_devices * capacity, D), jnp.bfloat16).at[own_slots].set(own_rows[token_of])
    )
    received = lax.all_to_all(
        outgoing.reshape(seq_devices, capacity, D), "sp", split_axis=0, concat_axis=0, tiled=True
    )
    gathered = lax.all_gather(received[:, None], "tp", axis=1, tiled=True)
    expert_in = gathered.reshape(-1, D)
    gate_part = jnp.dot(expert_in, w_gate[0], preferred_element_type=jnp.float32)
    up_part = jnp.dot(expert_in, w_up[0], preferred_element_type=jnp.float32)
    hidden = (jax.nn.silu(gate_part) * up_part).astype(jnp.bfloat16)
    partial_value = jnp.dot(hidden, w_down[0], preferred_element_type=jnp.float32)
    columns = lax.psum_scatter(
        partial_value.astype(jnp.bfloat16), "tp", scatter_dimension=1, tiled=True
    )
    col_count = columns.shape[1]
    returned = lax.all_to_all(
        columns.reshape(seq_devices, tp_devices * capacity, col_count),
        "sp",
        split_axis=0,
        concat_axis=0,
        tiled=True,
    )
    lookup = returned.reshape(-1, col_count)
    col_count = lookup.shape[1]
    picked = lookup[slots].reshape(row_count, 2, col_count).astype(jnp.float32)
    first_gate = group_weight * jax.nn.sigmoid(score_gap)
    second_gate = group_weight * jax.nn.sigmoid(-score_gap)
    result = middle_wide + first_gate[:, None] * picked[:, 0] + second_gate[:, None] * picked[:, 1]
    return result.astype(jnp.bfloat16)


def solution(mesh):
    return jax.shard_map(
        shards,
        mesh=mesh,
        in_specs=(
            P("sp", "tp"),
            P("sp", "tp"),
            P(None, "tp"),
            P("tp"),
            P("tp"),
            P("tp", None),
            P("sp", "tp"),
            P("tp"),
            P("sp", None),
            P("sp"),
            P("sp"),
            P("sp", None, "tp"),
            P("sp", None, "tp"),
            P("sp", "tp", None),
        ),
        out_specs=P("sp", "tp"),
        check_vma=False,
    )
```

profile of v0, /device:TPU:0, one launch (start us, length us, event | category | flops | bytes accessed | tf_op | source)
XLA Modules:
  0.0 363.9 jit_solution(2769100146873338767)
XLA Ops:
  6.5 0.8 slice.205
  7.4 4.9 %collective-permute-start = (bf16[30,256]{1,0:T(8,128)(2,1)S(1)}, bf16[30,256]{1,0:T(8,128)(2,1)S(1)}, u32[]{:S(2)}, u32[]{:S(2)}) collective-permute-start(bf16[30,256]{1,0:T(8,128)(2,1)S(1)} %slice.205), channel_id=1, source_target_pairs={{0,4},{4,8},{8,12},{12,16},{16,20},{20,24},{24,28},{1,5},{5,9},{9,... | collective-permute-start | bytes 46088 | tf_op jit(solution)/shard_map/ppermute | solution.py:14
  12.2 0.7 slice.206
  12.9 3.4 collective-permute-start.1
  16.4 1.0 fusion.62
  17.4 1.0 fusion.63
  18.4 1.2 divide_multiply_fusion
  19.7 0.0 copy-start.8
  19.7 0.0 copy-start.11
  19.7 0.0 copy-start.12
  19.7 2.4 fusion.59
  22.1 6.1 %all-reduce = (f32[512]{0:T(512)S(1)}, f32[512]{0:T(512)S(1)}) all-reduce(f32[512]{0:T(512)S(1)} %get-tuple-element.6, f32[512]{0:T(512)S(1)} %get-tuple-element.5), channel_id=1, replica_groups=mesh['sp'=8,'tp'=4] {'tp'}, use_global_device_ids=true, to_apply=%region_3.0 | all-reduce | flops 1024 | bytes 8192 | tf_op jit(solution)/shard_map/psum | solution.py:46
  28.2 2.1 convolution_convert_fusion.1
  30.3 0.0 reduce-scatter.3.cloned.1.call-update
  30.3 0.7 copy-done.4
  31.0 0.1 copy.18
  31.2 0.2 eq.26
  31.3 2.3 reduce-window.6
  33.6 0.1 slice.307
  33.7 0.1 copy.20
  33.8 29.0 %reduce-scatter.3.cloned.1.call-done = bf16[512,512]{1,0:T(8,128)(2,1)} async-done(((bf16[512,2048]{1,0:T(8,128)(2,1)}), bf16[512,512]{1,0:T(8,128)(2,1)}) %reduce-scatter.3.cloned.1.call-update) | async-done | bytes 524304 | tf_op jit(solution)/shard_map/reduce_scatter | solution.py:54
  62.9 1.3 fusion.1
  64.1 5.8 %psum.23 = f32[512]{0:T(512)S(1)} all-reduce(f32[512]{0:T(512)S(1)} %fusion.1), channel_id=1, replica_groups=mesh['sp'=8,'tp'=4] {'tp'}, use_global_device_ids=true, to_apply=%region_9.10 | all-reduce | flops 512 | bytes 4096 | tf_op jit(solution)/shard_map/psum | solution.py:59
  69.9 2.0 fusion.3
  72.0 3.5 all-to-all-start
  75.4 0.0 all-gather.3.cloned.1.call-start
  75.5 0.2 reshape.168
  75.7 0.1 fusion.53
  75.8 8.4 %all-to-all-done = bf16[4,128,512]{2,1,0:T(8,128)(2,1)S(1)} async-done(((bf16[4,128,512]{2,1,0:T(8,128)(2,1)}), bf16[4,128,512]{2,1,0:T(8,128)(2,1)S(1)}, u32[]{:S(2)}, u32[]{:S(2)}) %all-to-all-start) | async-done | bytes 524320 | tf_op jit(solution)/shard_map/all_to_all | solution.py:71
  84.2 0.9 copy.28
  85.1 6.4 %scatter_custom_fusion = bf16[512,2048]{1,0:T(8,128)(2,1)S(1)} fusion(s32[256]{0:T(256)S(1)} %bitcast.130, bf16[128,2048]{1,0:T(8,128)(2,1)} %bitcast.93, s32[1024]{0:T(1024)S(1)} %pad_clamp_fusion, bf16[]{:T(256)} %constant.25.clone.1), kind=kCustom, calls=%fused_computation.23 | custom fusion | bytes 2097664 | tf_op jit(solution)/shard_map/scatter | solution.py:78
  91.4 53.6 %all_to_all.29 = bf16[8,64,2048]{2,1,0:T(8,128)(2,1)} all-to-all(bf16[8,64,2048]{2,1,0:T(8,128)(2,1)S(1)} %bitcast.90), channel_id=1, replica_groups=mesh['sp'=8,'tp'=4] {'sp'}, dimensions={0} | all-to-all | bytes 4194304 | tf_op jit(solution)/shard_map/all_to_all | solution.py:80
  145.1 0.0 all-gather.3.cloned.1.call-update
  145.1 0.2 reduce-scatter.5.cloned.1.call-start
  145.3 56.4 %all-gather.3.cloned.1.call-done = bf16[8,256,2048]{2,1,0:T(8,128)(2,1)} async-done(((bf16[8,64,2048]{2,1,0:T(8,128)(2,1)}), bf16[8,256,2048]{2,1,0:T(8,128)(2,1)}) %all-gather.3.cloned.1.call-update) | async-done | bytes 8388624 | tf_op jit(solution)/shard_map/all_gather | solution.py:83
  201.7 7.2 %fusion.11 = f32[2048,256]{1,0:T(8,128)} fusion(bf16[2048,2048]{1,0:T(8,128)(2,1)} %bitcast.131, bf16[1,2048,256]{2,1,0:T(8,128)(2,1)S(1)} %copy-done.9), kind=kOutput, calls=%fused_computation.21 | convolution fusion | flops 2147483648 | bytes 11534336 | tf_op jit(solution)/shard_map/dot_general | solution.py:85
  208.9 13.1 %convolution_convert_fusion = bf16[2048,2048]{1,0:T(8,128)(2,1)} fusion(bf16[2048,2048]{1,0:T(8,128)(2,1)} %bitcast.132, f32[2048,256]{1,0:T(8,128)} %fusion.11, bf16[1,256,2048]{2,1,0:T(8,128)(2,1)S(1)} %copy-done, bf16[1,2048,256]{2,1,0:T(8,128)(2,1)S(1)} %copy-done.10), kind=kOutput, calls=%fused_computation.3 | convolution fusion | flops 4302307328 | bytes 20971520 | tf_op jit(solution)/shard_map/dot_general | solution.py:88
  222.0 0.0 reduce-scatter.5.cloned.1.call-update
  222.0 71.4 %reduce-scatter.5.cloned.1.call-done = bf16[2048,512]{1,0:T(8,128)(2,1)} async-done(((bf16[2048,2048]{1,0:T(8,128)(2,1)}), bf16[2048,512]{1,0:T(8,128)(2,1)}) %reduce-scatter.5.cloned.1.call-update) | async-done | bytes 2097168 | tf_op jit(solution)/shard_map/reduce_scatter | solution.py:89
  293.4 5.6 %all-to-all-start.2 = ((bf16[8,256,512]{2,1,0:T(8,128)(2,1)}), bf16[8,256,512]{2,1,0:T(8,128)(2,1)S(1)}, u32[]{:S(2)}, u32[]{:S(2)}) async-start(bf16[8,256,512]{2,1,0:T(8,128)(2,1)} %bitcast.91), calls=%async_computation.4 | async-start | bytes 4194304 | tf_op jit(solution)/shard_map/all_to_all | solution.py:93
  299.1 0.1 copy.23
  299.2 0.2 mul.551
  299.5 47.6 %all-to-all-done.2 = bf16[8,256,512]{2,1,0:T(8,128)(2,1)S(1)} async-done(((bf16[8,256,512]{2,1,0:T(8,128)(2,1)}), bf16[8,256,512]{2,1,0:T(8,128)(2,1)S(1)}, u32[]{:S(2)}, u32[]{:S(2)}) %all-to-all-start.2) | async-done | bytes 2097184 | tf_op jit(solution)/shard_map/all_to_all | solution.py:93
  347.2 5.0 %gather_fusion = bf16[1024,512]{1,0:T(8,128)(2,1)} fusion(bf16[2048,512]{1,0:T(8,128)(2,1)S(1)} %bitcast.89, s32[1024]{0:T(1024)S(1)} %broadcast_clamp_fusion), kind=kCustom, calls=%fused_computation.1 | custom fusion | bytes 2101248 | tf_op jit(solution)/shard_map/gather | solution.py:102
  352.2 2.4 reshape.174
  354.6 0.0 copy-start.2
  354.6 1.6 fusion.61
  356.3 1.1 fusion.5
  (40 shorter events, 0.2 us)
Async XLA Ops:
  6.5 202.4 %copy-start = (bf16[1,256,2048]{2,1,0:T(8,128)(2,1)S(1)}, bf16[1,256,2048]{2,1,0:T(8,128)(2,1)}, u32[]{:S(2)}) copy-start(bf16[1,256,2048]{2,1,0:T(8,128)(2,1)} %param.27) | copy-start | bytes 3145732
  6.5 56.3 %reduce-scatter.3.cloned.1.call-start = ((), (), s32[]{:S(2)}) async-start(), calls=%async_computation.5 | async-start | bytes 2621440 | tf_op jit(solution)/shard_map/reduce_scatter | solution.py:54
  7.4 11.1 %collective-permute-start = (bf16[30,256]{1,0:T(8,128)(2,1)S(1)}, bf16[30,256]{1,0:T(8,128)(2,1)S(1)}, u32[]{:S(2)}, u32[]{:S(2)}) collective-permute-start(bf16[30,256]{1,0:T(8,128)(2,1)S(1)} %slice.205), channel_id=1, source_target_pairs={{0,4},{4,8},{8,12},{12,16},{16,20},{20,24},{24,28},{1,5},{5,9},{9,... | collective-permute-start | bytes 46088 | tf_op jit(solution)/shard_map/ppermute | solution.py:14
  12.9 5.5 %collective-permute-start.1 = (bf16[30,256]{1,0:T(8,128)(2,1)S(1)}, bf16[30,256]{1,0:T(8,128)(2,1)S(1)}, u32[]{:S(2)}, u32[]{:S(2)}) collective-permute-start(bf16[30,256]{1,0:T(8,128)(2,1)S(1)} %slice.206), channel_id=1, source_target_pairs={{0,4},{4,8},{8,12},{12,16},{16,20},{20,24},{24,28},{1,5},{5,9},{9,... | collective-permute-start | bytes 46088 | tf_op jit(solution)/shard_map/ppermute | solution.py:14
  19.7 8.5 %copy-start.8 = (bf16[256,2048]{1,0:T(8,128)(2,1)S(1)}, bf16[256,2048]{1,0:T(8,128)(2,1)}, u32[]{:S(2)}) copy-start(bf16[256,2048]{1,0:T(8,128)(2,1)} %param.19) | copy-start | bytes 3145732
  19.7 8.5 %copy-start.11 = (f32[256]{0:T(256)S(1)}, f32[256]{0:T(256)}, u32[]{:S(2)}) copy-start(f32[256]{0:T(256)} %param.18) | copy-start | bytes 3076
  19.7 8.5 %copy-start.12 = (f32[256]{0:T(256)S(1)}, f32[256]{0:T(256)}, u32[]{:S(2)}) copy-start(f32[256]{0:T(256)} %param.17) | copy-start | bytes 3076
  30.3 0.7 copy-start.4
  30.3 32.5 %copy-start.1 = (bf16[512,512]{1,0:T(8,128)(2,1)S(1)}, bf16[512,512]{1,0:T(8,128)(2,1)}, u32[]{:S(2)}) copy-start(bf16[512,512]{1,0:T(8,128)(2,1)} %param.20) | copy-start | bytes 1572868
  30.3 39.6 %copy-start.5 = (f32[512]{0:T(512)S(1)}, f32[512]{0:T(512)}, u32[]{:S(2)}) copy-start(f32[512]{0:T(512)} %param.21) | copy-start | bytes 6148
  72.0 12.3 %all-to-all-start = ((bf16[4,128,512]{2,1,0:T(8,128)(2,1)}), bf16[4,128,512]{2,1,0:T(8,128)(2,1)S(1)}, u32[]{:S(2)}, u32[]{:S(2)}) async-start(bf16[4,128,512]{2,1,0:T(8,128)(2,1)} %bitcast.36), calls=%async_computation.1 | async-start | bytes 1048576 | tf_op jit(solution)/shard_map/all_to_all | solution.py:71
  75.4 126.3 %all-gather.3.cloned.1.call-start = ((), (), s32[]{:S(2)}) async-start(), calls=%async_computation.7 | async-start | bytes 10485760 | tf_op jit(solution)/shard_map/all_gather | solution.py:83
  145.1 56.7 %copy-start.9 = (bf16[1,2048,256]{2,1,0:T(8,128)(2,1)S(1)}, bf16[1,2048,256]{2,1,0:T(8,128)(2,1)}, u32[]{:S(2)}) copy-start(bf16[1,2048,256]{2,1,0:T(8,128)(2,1)} %param.25) | copy-start | bytes 3145732
  145.1 148.3 %reduce-scatter.5.cloned.1.call-start = ((), (), s32[]{:S(2)}) async-start(), calls=%async_computation.6 | async-start | bytes 10485760 | tf_op jit(solution)/shard_map/reduce_scatter | solution.py:89
  201.7 7.2 %copy-start.10 = (bf16[1,2048,256]{2,1,0:T(8,128)(2,1)S(1)}, bf16[1,2048,256]{2,1,0:T(8,128)(2,1)}, u32[]{:S(2)}) copy-start(bf16[1,2048,256]{2,1,0:T(8,128)(2,1)} %param.26) | copy-start | bytes 3145732
  293.4 6.1 %copy-start.6 = (f32[512]{0:T(512)S(1)}, f32[512]{0:T(512)}, u32[]{:S(2)}) copy-start(f32[512]{0:T(512)} %param.23) | copy-start | bytes 6148
  293.4 6.1 %copy-start.7 = (f32[512]{0:T(512)S(1)}, f32[512]{0:T(512)}, u32[]{:S(2)}) copy-start(f32[512]{0:T(512)} %param.24) | copy-start | bytes 6148
  293.4 53.7 %all-to-all-start.2 = ((bf16[8,256,512]{2,1,0:T(8,128)(2,1)}), bf16[8,256,512]{2,1,0:T(8,128)(2,1)S(1)}, u32[]{:S(2)}, u32[]{:S(2)}) async-start(bf16[8,256,512]{2,1,0:T(8,128)(2,1)} %bitcast.91), calls=%async_computation.4 | async-start | bytes 4194304 | tf_op jit(solution)/shard_map/all_to_all | solution.py:93
  354.6 1.7 copy-start.2
  354.6 1.6 copy-start.3
Sparse Core Ops, SparseCore 0:
  30.5 32.3 reduce-scatter.2
  145.2 56.4 all-gather.2
  222.2 71.2 reduce-scatter.4
where the time goes:
time: 365 us; the launch traced here: 364 us
  waiting for transfers between devices  213 us (58%)
  blocking collectives  65.4 us (18%)
  matrix products  22.4 us (6%)
  local copies, waits for them, and re-layouts  21.5 us (6%)
  starting transfers between devices  17.7 us (5%)
  between operations  13.4 us (4%)
  other arithmetic  10.5 us (3%)
    reduce_scatter x1, waiting for transfers between devices, shards(): lax.psum_scatter(partial_value.astype(jnp.bfloat16), 'tp', scatter_dimens...  71.4 us
    all_gather x1, waiting for transfers between devices, shards(): gathered = lax.all_gather(received[:, None], 'tp', axis=1, tiled=True)  56.4 us
    all_to_all x1, blocking collectives, shards(): lax.all_to_all(outgoing.reshape(seq_devices, capacity, D), 'sp', split_ax...  53.6 us
    all_to_all x1, waiting for transfers between devices, shards(): lax.all_to_all(columns.reshape(seq_devices, tp_devices * capacity, col_co...  47.6 us
    reduce_scatter x1, waiting for transfers between devices, shards(): lax.psum_scatter(partial_out.astype(jnp.bfloat16), 'tp', scatter_dimensio...  29 us
    dot_general x1, matrix products, shards(): jnp.dot(hidden, w_down[0], preferred_element_type=jnp.float32)  13.1 us
    all_to_all x1, waiting for transfers between devices, shards(): lax.all_to_all(normed, 'tp', split_axis=0, concat_axis=1, tiled=True)  8.4 us
    ppermute x2, starting transfers between devices, passed_along(): lax.ppermute(value, axis, [(source, source + steps) for source in range(l...  8.3 us
  transfers between devices with their start and end apart: 7, of which 5 were waited for; matrix products, arithmetic and copies ran while one was open for 2% of the time, Pallas kernels for 0%

commit v1 on v0

--- a/solution.py
+++ b/solution.py
@@ -80,7 +80,9 @@
     received = lax.all_to_all(
         outgoing.reshape(seq_devices, capacity, D), "sp", split_axis=0, concat_axis=0, tiled=True
     )
-    gathered = lax.all_gather(received[:, None], "tp", axis=1, tiled=True)
+    x = received[:, None]
+    blocks = lax.all_gather(x, "tp")
+    gathered = jnp.concatenate(blocks, axis=1)
     expert_in = gathered.reshape(-1, D)
     gate_part = jnp.dot(expert_in, w_gate[0], preferred_element_type=jnp.float32)
     up_part = jnp.dot(expert_in, w_up[0], preferred_element_type=jnp.float32)

time: 365 us -> 373 us (1.022)
  local copies, waits for them, and re-layouts: 21.5 us -> 29.9 us
    reshape x0 -> x1, local copies, waits for them, and re-layouts: none -> 8.35 us  [shards(): gathered = jnp.concatenate(blocks, axis=1)]
where the time goes in v1:
time: 373 us; the launch traced here: 372 us
  waiting for transfers between devices  213 us (57%)
  blocking collectives  65.4 us (18%)
  local copies, waits for them, and re-layouts  29.9 us (8%)
  matrix products  22.4 us (6%)
  starting transfers between devices  17.7 us (5%)
  between operations  13.4 us (4%)
  other arithmetic  10.5 us (3%)
    reduce_scatter x1, waiting for transfers between devices, shards(): lax.psum_scatter(partial_value.astype(jnp.bfloat16), 'tp', scatter_dimens...  71.4 us
    all_gather x1, waiting for transfers between devices, shards(): blocks = lax.all_gather(x, 'tp')  56.4 us
    all_to_all x1, blocking collectives, shards(): lax.all_to_all(outgoing.reshape(seq_devices, capacity, D), 'sp', split_ax...  53.6 us
    all_to_all x1, waiting for transfers between devices, shards(): lax.all_to_all(columns.reshape(seq_devices, tp_devices * capacity, col_co...  47.6 us
    reduce_scatter x1, waiting for transfers between devices, shards(): lax.psum_scatter(partial_out.astype(jnp.bfloat16), 'tp', scatter_dimensio...  29 us
    dot_general x1, matrix products, shards(): jnp.dot(hidden, w_down[0], preferred_element_type=jnp.float32)  13.1 us
    all_to_all x1, waiting for transfers between devices, shards(): lax.all_to_all(normed, 'tp', split_axis=0, concat_axis=1, tiled=True)  8.4 us
    reshape x1, local copies, waits for them, and re-layouts, shards(): gathered = jnp.concatenate(blocks, axis=1)  8.35 us
  transfers between devices with their start and end apart: 7, of which 5 were waited for; matrix products, arithmetic and copies ran while one was open for 2% of the time, Pallas kernels for 0%

profile of v1, /device:TPU:0, one launch (start us, length us, event | category | flops | bytes accessed | tf_op | source)
XLA Modules:
  0.0 372.2 jit_solution(5035283773459256999)
XLA Ops:
  6.5 0.8 slice.205
  7.4 4.9 %collective-permute-start = (bf16[30,256]{1,0:T(8,128)(2,1)S(1)}, bf16[30,256]{1,0:T(8,128)(2,1)S(1)}, u32[]{:S(2)}, u32[]{:S(2)}) collective-permute-start(bf16[30,256]{1,0:T(8,128)(2,1)S(1)} %slice.205), channel_id=1, source_target_pairs={{0,4},{4,8},{8,12},{12,16},{16,20},{20,24},{24,28},{1,5},{5,9},{9,... | collective-permute-start | bytes 46088 | tf_op jit(solution)/shard_map/ppermute | solution.py:14
  12.2 0.7 slice.206
  12.9 3.4 collective-permute-start.1
  16.4 1.0 fusion.62
  17.4 1.0 fusion.63
  18.4 1.2 divide_multiply_fusion
  19.7 0.0 copy-start.8
  19.7 0.0 copy-start.11
  19.7 2.4 fusion.59
  22.1 6.1 %all-reduce = (f32[512]{0:T(512)S(1)}, f32[512]{0:T(512)S(1)}) all-reduce(f32[512]{0:T(512)S(1)} %get-tuple-element.6, f32[512]{0:T(512)S(1)} %get-tuple-element.5), channel_id=1, replica_groups=mesh['sp'=8,'tp'=4] {'tp'}, use_global_device_ids=true, to_apply=%region_3.0 | all-reduce | flops 1024 | bytes 8192 | tf_op jit(solution)/shard_map/psum | solution.py:46
  28.2 2.1 convolution_convert_fusion.1
  30.3 0.0 reduce-scatter.3.cloned.1.call-update
  30.3 0.7 copy-done.4
  31.0 0.1 copy.35
  31.2 0.2 eq.26
  31.3 2.3 reduce-window.6
  33.6 0.1 slice.307
  33.7 0.1 copy.37
  33.8 29.0 %reduce-scatter.3.cloned.1.call-done = bf16[512,512]{1,0:T(8,128)(2,1)} async-done(((bf16[512,2048]{1,0:T(8,128)(2,1)}), bf16[512,512]{1,0:T(8,128)(2,1)}) %reduce-scatter.3.cloned.1.call-update) | async-done | bytes 524304 | tf_op jit(solution)/shard_map/reduce_scatter | solution.py:54
  62.9 1.3 fusion.1
  64.1 5.8 %psum.23 = f32[512]{0:T(512)S(1)} all-reduce(f32[512]{0:T(512)S(1)} %fusion.1), channel_id=1, replica_groups=mesh['sp'=8,'tp'=4] {'tp'}, use_global_device_ids=true, to_apply=%region_9.10 | all-reduce | flops 512 | bytes 4096 | tf_op jit(solution)/shard_map/psum | solution.py:59
  69.9 2.0 fusion.3
  72.0 3.5 all-to-all-start
  75.4 0.0 all-gather.3.cloned.1.call-start
  75.5 0.2 reshape.168
  75.7 0.1 fusion.53
  75.8 8.4 %all-to-all-done = bf16[4,128,512]{2,1,0:T(8,128)(2,1)S(1)} async-done(((bf16[4,128,512]{2,1,0:T(8,128)(2,1)}), bf16[4,128,512]{2,1,0:T(8,128)(2,1)S(1)}, u32[]{:S(2)}, u32[]{:S(2)}) %all-to-all-start) | async-done | bytes 524320 | tf_op jit(solution)/shard_map/all_to_all | solution.py:71
  84.2 0.9 copy.46
  85.1 6.4 %scatter_custom_fusion = bf16[512,2048]{1,0:T(8,128)(2,1)S(1)} fusion(s32[256]{0:T(256)S(1)} %bitcast.136, bf16[128,2048]{1,0:T(8,128)(2,1)} %bitcast.99, s32[1024]{0:T(1024)S(1)} %pad_clamp_fusion, bf16[]{:T(256)} %constant.25.clone.1), kind=kCustom, calls=%fused_computation.23 | custom fusion | bytes 2097664 | tf_op jit(solution)/shard_map/scatter | solution.py:78
  91.4 53.6 %all_to_all.29 = bf16[8,64,2048]{2,1,0:T(8,128)(2,1)} all-to-all(bf16[8,64,2048]{2,1,0:T(8,128)(2,1)S(1)} %bitcast.96), channel_id=1, replica_groups=mesh['sp'=8,'tp'=4] {'sp'}, dimensions={0} | all-to-all | bytes 4194304 | tf_op jit(solution)/shard_map/all_to_all | solution.py:80
  145.1 0.0 all-gather.3.cloned.1.call-update
  145.1 0.2 reduce-scatter.5.cloned.1.call-start
  145.3 56.4 %all-gather.3.cloned.1.call-done = bf16[32,64,2048]{2,1,0:T(8,128)(2,1)} async-done(((bf16[8,64,2048]{2,1,0:T(8,128)(2,1)}), bf16[32,64,2048]{2,1,0:T(8,128)(2,1)}) %all-gather.3.cloned.1.call-update) | async-done | bytes 8388624 | tf_op jit(solution)/shard_map/all_gather | solution.py:84
  201.7 8.4 %copy.40 = bf16[8,4,1,64,2048]{4,3,1,0,2:T(8,128)(2,1)} copy(bf16[8,4,1,64,2048]{4,3,0,1,2:T(8,128)(2,1)} %bitcast.93) | data formatting | bytes 16777216 | tf_op jit(solution)/shard_map/reshape | solution.py:85
  210.1 7.2 %fusion.11 = f32[2048,256]{1,0:T(8,128)} fusion(bf16[2048,2048]{1,0:T(8,128)(2,1)} %bitcast.94, bf16[1,2048,256]{2,1,0:T(8,128)(2,1)S(1)} %copy-done.9), kind=kOutput, calls=%fused_computation.21 | convolution fusion | flops 2147483648 | bytes 11534336 | tf_op jit(solution)/shard_map/dot_general | solution.py:87
  217.3 13.1 %convolution_convert_fusion = bf16[2048,2048]{1,0:T(8,128)(2,1)} fusion(bf16[2048,2048]{1,0:T(8,128)(2,1)} %bitcast.95, f32[2048,256]{1,0:T(8,128)} %fusion.11, bf16[1,256,2048]{2,1,0:T(8,128)(2,1)S(1)} %copy-done, bf16[1,2048,256]{2,1,0:T(8,128)(2,1)S(1)} %copy-done.10), kind=kOutput, calls=%fused_computation.3 | convolution fusion | flops 4302307328 | bytes 20971520 | tf_op jit(solution)/shard_map/dot_general | solution.py:90
  230.4 0.0 reduce-scatter.5.cloned.1.call-update
  230.4 71.4 %reduce-scatter.5.cloned.1.call-done = bf16[2048,512]{1,0:T(8,128)(2,1)} async-done(((bf16[2048,2048]{1,0:T(8,128)(2,1)}), bf16[2048,512]{1,0:T(8,128)(2,1)}) %reduce-scatter.5.cloned.1.call-update) | async-done | bytes 2097168 | tf_op jit(solution)/shard_map/reduce_scatter | solution.py:91
  301.8 5.6 %all-to-all-start.2 = ((bf16[8,256,512]{2,1,0:T(8,128)(2,1)}), bf16[8,256,512]{2,1,0:T(8,128)(2,1)S(1)}, u32[]{:S(2)}, u32[]{:S(2)}) async-start(bf16[8,256,512]{2,1,0:T(8,128)(2,1)} %bitcast.97), calls=%async_computation.4 | async-start | bytes 4194304 | tf_op jit(solution)/shard_map/all_to_all | solution.py:95
  307.5 0.1 copy.41
  307.6 0.2 mul.551
  307.9 47.6 %all-to-all-done.2 = bf16[8,256,512]{2,1,0:T(8,128)(2,1)S(1)} async-done(((bf16[8,256,512]{2,1,0:T(8,128)(2,1)}), bf16[8,256,512]{2,1,0:T(8,128)(2,1)S(1)}, u32[]{:S(2)}, u32[]{:S(2)}) %all-to-all-start.2) | async-done | bytes 2097184 | tf_op jit(solution)/shard_map/all_to_all | solution.py:95
  355.5 5.0 %gather_fusion = bf16[1024,512]{1,0:T(8,128)(2,1)} fusion(bf16[2048,512]{1,0:T(8,128)(2,1)S(1)} %bitcast.92, s32[1024]{0:T(1024)S(1)} %broadcast_clamp_fusion), kind=kCustom, calls=%fused_computation.1 | custom fusion | bytes 2101248 | tf_op jit(solution)/shard_map/gather | solution.py:104
  360.6 2.4 reshape.174
  363.0 0.0 copy-start.2
  363.0 1.6 fusion.61
  364.6 1.1 fusion.5
  (41 shorter events, 0.2 us)
Async XLA Ops:
  6.5 210.7 %copy-start = (bf16[1,256,2048]{2,1,0:T(8,128)(2,1)S(1)}, bf16[1,256,2048]{2,1,0:T(8,128)(2,1)}, u32[]{:S(2)}) copy-start(bf16[1,256,2048]{2,1,0:T(8,128)(2,1)} %param.27) | copy-start | bytes 3145732
  6.5 56.3 %reduce-scatter.3.cloned.1.call-start = ((), (), s32[]{:S(2)}) async-start(), calls=%async_computation.5 | async-start | bytes 2621440 | tf_op jit(solution)/shard_map/reduce_scatter | solution.py:54
  7.4 11.1 %collective-permute-start = (bf16[30,256]{1,0:T(8,128)(2,1)S(1)}, bf16[30,256]{1,0:T(8,128)(2,1)S(1)}, u32[]{:S(2)}, u32[]{:S(2)}) collective-permute-start(bf16[30,256]{1,0:T(8,128)(2,1)S(1)} %slice.205), channel_id=1, source_target_pairs={{0,4},{4,8},{8,12},{12,16},{16,20},{20,24},{24,28},{1,5},{5,9},{9,... | collective-permute-start | bytes 46088 | tf_op jit(solution)/shard_map/ppermute | solution.py:14
  12.9 5.5 %collective-permute-start.1 = (bf16[30,256]{1,0:T(8,128)(2,1)S(1)}, bf16[30,256]{1,0:T(8,128)(2,1)S(1)}, u32[]{:S(2)}, u32[]{:S(2)}) collective-permute-start(bf16[30,256]{1,0:T(8,128)(2,1)S(1)} %slice.206), channel_id=1, source_target_pairs={{0,4},{4,8},{8,12},{12,16},{16,20},{20,24},{24,28},{1,5},{5,9},{9,... | collective-permute-start | bytes 46088 | tf_op jit(solution)/shard_map/ppermute | solution.py:14
  19.7 8.5 %copy-start.8 = (bf16[256,2048]{1,0:T(8,128)(2,1)S(1)}, bf16[256,2048]{1,0:T(8,128)(2,1)}, u32[]{:S(2)}) copy-start(bf16[256,2048]{1,0:T(8,128)(2,1)} %param.19) | copy-start | bytes 3145732
  19.7 8.5 %copy-start.11 = (f32[256]{0:T(256)S(1)}, f32[256]{0:T(256)}, u32[]{:S(2)}) copy-start(f32[256]{0:T(256)} %param.18) | copy-start | bytes 3076
  19.7 8.5 %copy-start.12 = (f32[256]{0:T(256)S(1)}, f32[256]{0:T(256)}, u32[]{:S(2)}) copy-start(f32[256]{0:T(256)} %param.17) | copy-start | bytes 3076
  30.3 0.7 copy-start.4
  30.3 32.5 %copy-start.1 = (bf16[512,512]{1,0:T(8,128)(2,1)S(1)}, bf16[512,512]{1,0:T(8,128)(2,1)}, u32[]{:S(2)}) copy-start(bf16[512,512]{1,0:T(8,128)(2,1)} %param.20) | copy-start | bytes 1572868
  30.3 39.6 %copy-start.5 = (f32[512]{0:T(512)S(1)}, f32[512]{0:T(512)}, u32[]{:S(2)}) copy-start(f32[512]{0:T(512)} %param.21) | copy-start | bytes 6148
  72.0 12.3 %all-to-all-start = ((bf16[4,128,512]{2,1,0:T(8,128)(2,1)}), bf16[4,128,512]{2,1,0:T(8,128)(2,1)S(1)}, u32[]{:S(2)}, u32[]{:S(2)}) async-start(bf16[4,128,512]{2,1,0:T(8,128)(2,1)} %bitcast.36), calls=%async_computation.1 | async-start | bytes 1048576 | tf_op jit(solution)/shard_map/all_to_all | solution.py:71
  75.4 126.3 %all-gather.3.cloned.1.call-start = ((), (), s32[]{:S(2)}) async-start(), calls=%async_computation.7 | async-start | bytes 10485760 | tf_op jit(solution)/shard_map/all_gather | solution.py:84
  145.1 156.7 %reduce-scatter.5.cloned.1.call-start = ((), (), s32[]{:S(2)}) async-start(), calls=%async_computation.6 | async-start | bytes 10485760 | tf_op jit(solution)/shard_map/reduce_scatter | solution.py:91
  201.7 8.4 %copy-start.9 = (bf16[1,2048,256]{2,1,0:T(8,128)(2,1)S(1)}, bf16[1,2048,256]{2,1,0:T(8,128)(2,1)}, u32[]{:S(2)}) copy-start(bf16[1,2048,256]{2,1,0:T(8,128)(2,1)} %param.25) | copy-start | bytes 3145732
  210.1 7.2 %copy-start.10 = (bf16[1,2048,256]{2,1,0:T(8,128)(2,1)S(1)}, bf16[1,2048,256]{2,1,0:T(8,128)(2,1)}, u32[]{:S(2)}) copy-start(bf16[1,2048,256]{2,1,0:T(8,128)(2,1)} %param.26) | copy-start | bytes 3145732
  301.8 6.1 %copy-start.6 = (f32[512]{0:T(512)S(1)}, f32[512]{0:T(512)}, u32[]{:S(2)}) copy-start(f32[512]{0:T(512)} %param.23) | copy-start | bytes 6148
  301.8 6.1 %copy-start.7 = (f32[512]{0:T(512)S(1)}, f32[512]{0:T(512)}, u32[]{:S(2)}) copy-start(f32[512]{0:T(512)} %param.24) | copy-start | bytes 6148
  301.8 53.7 %all-to-all-start.2 = ((bf16[8,256,512]{2,1,0:T(8,128)(2,1)}), bf16[8,256,512]{2,1,0:T(8,128)(2,1)S(1)}, u32[]{:S(2)}, u32[]{:S(2)}) async-start(bf16[8,256,512]{2,1,0:T(8,128)(2,1)} %bitcast.97), calls=%async_computation.4 | async-start | bytes 4194304 | tf_op jit(solution)/shard_map/all_to_all | solution.py:95
  363.0 1.7 copy-start.2
  363.0 1.6 copy-start.3
Sparse Core Ops, SparseCore 0:
  30.5 32.3 reduce-scatter.2
  145.2 56.4 all-gather.2
  230.5 71.2 reduce-scatter.4
